TPU v7x, 256 devices: a whole 4x4x8 slice. The times are simulated.
256 devices in a mesh: rep: 2 (over z_hi), fs: 16 (over z_lo, y), tp: 8 (over x, core).
Axes of the slice: x: 4, y: 4, z: 8 (z_hi: 2, z_lo: 4; z = z_hi * 4 + z_lo), core: 2. Of those that a mesh axis runs over, the one named last changes fastest.
Arguments:
- stream: bfloat16 [32768, 2048], P(('rep', 'fs', 'tp')), may hold values from -6 to 6
- gain_before: float32 [2048], replicated, may hold values from 0.1 to 1.9
- gain_after: float32 [2048], replicated, may hold values from 0.1 to 1.9
- proj_gate: bfloat16 [2048, 3584], P('fs', 'tp'), may hold values from -0.125 to 0.125
- proj_lift: bfloat16 [2048, 3584], P('fs', 'tp'), may hold values from -0.125 to 0.125
- proj_down: bfloat16 [3584, 2048], P('tp', 'fs'), may hold values from -0.09375 to 0.09375
- mixer_gain: float32 [2048], replicated, may hold values from 0.1 to 1.9
- mixer_u: bfloat16 [2048, 2048], P('fs', 'tp'), may hold values from -0.125 to 0.125
- mixer_v: bfloat16 [2048, 2048], P('fs', 'tp'), may hold values from -1 to 1
- layer_gain: float32 [2048], P('tp'), may hold values from 0.1 to 1.9
- layer_shift: float32 [2048], P('tp'), may hold values from -3 to 3
- spatial: bfloat16 [16, 128, 128], P('tp'), may hold values from -0.5 to 0.5
- spatial_shift: float32 [16, 128], P('tp'), may hold values from 0.2 to 2
- mixer_down: bfloat16 [2048, 2048], P('tp', 'fs'), may hold values from -0.125 to 0.125
Outputs:
- result: bfloat16 [32768, 2048], P(('rep', 'fs', 'tp'))
All inputs are finite; a program needn't handle non-finite values.
Results may differ from a plain program's by a relative error of at most 0.017.
Values may be sent and summed in bfloat16 or wider, within the bound.
A program may use at most 128 MiB of HBM per device.

v0:
```python
import jax
import jax.numpy as jnp
from jax import lax
from jax.sharding import PartitionSpec as P

GROUP_DIM = 128
SPAN = 128
A = 2048
norm_epsilon = 1e-06
layer_epsilon = 1e-05


def sent_to_all(value, axis):
    copies = jnp.broadcast_to(value, (lax.axis_size(axis), *value.shape))
    return lax.all_to_all(copies, axis, split_axis=0, concat_axis=0, tiled=True)


def laid_out(tiles, dim):
    lengths = list(tiles.shape[1:])
    lengths[dim] *= tiles.shape[0]
    return jnp.moveaxis(tiles, 0, dim).reshape(lengths)


def gathered_copies(value, axis, dim):
    tiles = sent_to_all(value, axis)
    return laid_out(tiles, dim)


def side_by_side(arrays, axis, dim, along):
    ends, at = ([], 0)
    for a in arrays[:-1]:
        at += a.shape[along]
        ends.append(at)
    both = jnp.concatenate(arrays, axis=along)
    return tuple(jnp.split(lax.all_gather(both, axis, axis=dim, tiled=True), ends, axis=along))


def norm_rows(row_block, scale_gain):
    widened = row_block.astype(jnp.float32)
    factor = lax.rsqrt(jnp.mean(widened * widened, axis=1, keepdims=True) + norm_epsilon)
    return (widened * factor * scale_gain).astype(jnp.bfloat16)


def gathered_norm(stream_rows, scale_gain):
    gathered = lax.all_gather(stream_rows, "tp", axis=0, tiled=True)
    return norm_rows(gathered, scale_gain)


def pair_adder(normed, pieces):
    return (
        jnp.dot(normed, pieces[0], preferred_element_type=jnp.float32),
        jnp.dot(normed, pieces[1], preferred_element_type=jnp.float32),
    )


def activate(gate_vals, lift_vals):
    return (jax.nn.silu(gate_vals) * lift_vals).astype(jnp.bfloat16)


def rows_project(columns_here, weight_shard):
    weight_cols = gathered_copies(weight_shard, "fs", 1)
    weight_whole = lax.all_gather(weight_cols, "tp", axis=0, tiled=True)
    own_tokens = lax.all_to_all(columns_here, "tp", split_axis=0, concat_axis=1, tiled=True)
    width = columns_here.shape[1]
    running = jnp.zeros((own_tokens.shape[0], weight_whole.shape[1]), jnp.float32)
    for member in range(lax.axis_size("tp")):
        partial_value = jnp.dot(
            own_tokens[:, member * width : (member + 1) * width],
            weight_whole[member * width : (member + 1) * width],
            preferred_element_type=jnp.float32,
        )
        running = running + partial_value.astype(jnp.bfloat16).astype(jnp.float32)
    return running


def half_kept(stream_rows, scale_gain, gate_whole, lift_whole, proj_down):
    normed = gathered_norm(stream_rows, scale_gain)
    gate_vals = jnp.dot(normed, gate_whole, preferred_element_type=jnp.float32)
    lift_vals = jnp.dot(normed, lift_whole, preferred_element_type=jnp.float32)
    hidden = activate(gate_vals, lift_vals)
    summed = rows_project(hidden, proj_down)
    return (stream_rows.astype(jnp.float32) + 0.5 * summed).astype(jnp.bfloat16)


def token_mixer(
    stream_rows,
    mixer_gain,
    mixer_u,
    mixer_v,
    layer_gain,
    layer_shift,
    spatial,
    spatial_shift,
    mixer_down,
):
    gathered = lax.all_gather(stream_rows, "tp", axis=0, tiled=True)
    normed = norm_rows(gathered, mixer_gain)
    seq_tokens = normed.shape[0]
    u_vals, v_vals = pair_adder(normed, side_by_side((mixer_u, mixer_v), "fs", 0, 1))
    lifted = jax.nn.gelu(v_vals)
    moments = lax.psum((jnp.sum(lifted, axis=1), jnp.sum(lifted * lifted, axis=1)), "tp")
    centre = moments[0] / A
    spread = moments[1] / A - centre * centre
    normed_v = (
        (lifted - centre[:, None]) * lax.rsqrt(spread[:, None] + layer_epsilon) * layer_gain
        + layer_shift
    ).astype(jnp.bfloat16)
    groups_here = spatial.shape[0]
    blocked = normed_v.reshape(seq_tokens // SPAN, SPAN, groups_here, GROUP_DIM)
    causal = jnp.tril(jnp.ones((SPAN, SPAN), dtype=bool))
    masked = jnp.where(causal[None], spatial, jnp.zeros((), jnp.bfloat16))
    mixed_v = jnp.einsum("gts,bsgd->btgd", masked, blocked, preferred_element_type=jnp.float32)
    mixed_v = mixed_v + spatial_shift.T[None, :, :, None]
    gated = (jax.nn.gelu(u_vals) * mixed_v.reshape(seq_tokens, groups_here * GROUP_DIM)).astype(
        jnp.bfloat16
    )
    summed = rows_project(gated, mixer_down)
    return (stream_rows.astype(jnp.float32) + summed).astype(jnp.bfloat16)


def body(
    stream,
    gain_before,
    gain_after,
    proj_gate,
    proj_lift,
    proj_down,
    mixer_gain,
    mixer_u,
    mixer_v,
    layer_gain,
    layer_shift,
    spatial,
    spatial_shift,
    mixer_down,
):
    gate_whole, lift_whole = side_by_side((proj_gate, proj_lift), "fs", 0, 1)
    first = half_kept(stream, gain_before, gate_whole, lift_whole, proj_down)
    second = token_mixer(
        first,
        mixer_gain,
        mixer_u,
        mixer_v,
        layer_gain,
        layer_shift,
        spatial,
        spatial_shift,
        mixer_down,
    )
    result = half_kept(second, gain_after, gate_whole, lift_whole, proj_down)
    return result


def solution(mesh):
    placed = (
        P(("rep", "fs", "tp"), None),
        P(),
        P(),
        P("fs", "tp"),
        P("fs", "tp"),
        P("tp", "fs"),
        P(),
        P("fs", "tp"),
        P("fs", "tp"),
        P("tp"),
        P("tp"),
        P("tp", None, None),
        P("tp", None),
        P("tp", "fs"),
    )
    return jax.shard_map(
        body, mesh=mesh, in_specs=placed, out_specs=P(("rep", "fs", "tp"), None), check_vma=False
    )
```

profile of v0, /device:TPU:1, one launch (start us, length us, event | category | flops | bytes accessed | tf_op | source)
XLA Modules:
  0.0 495.1 jit_solution(2137628182025998506)
XLA Ops:
  6.5 0.7 all-gather.8.cloned.1.call-update
  7.3 1.7 pad_maximum_fusion
  9.0 1.2 broadcast_in_dim.14
  10.3 51.8 %all_to_all.68 = bf16[16,448,128]{2,1,0:T(8,128)(2,1)S(1)} all-to-all(bf16[16,448,128]{2,1,0:T(8,128)(2,1)S(1)} %broadcast_in_dim.14), channel_id=1, replica_groups=mesh['rep'=2,'fs'=16,'tp'=8] {'fs'}, dimensions={0} | all-to-all | bytes 3670016 | tf_op jit(solution)/shard_map/all_to_all | solution.py:15
  62.1 1.5 copy_bitcast_fusion
  63.7 3.1 fusion
  66.8 58.1 %all-gather.10.cloned.1.call-done = bf16[2048,896]{0,1:T(8,128)(2,1)} async-done(((bf16[128,896]{0,1:T(8,128)(2,1)}), bf16[2048,896]{0,1:T(8,128)(2,1)}) %all-gather.10.cloned.1.call-update) | async-done | bytes 3670032 | tf_op jit(solution)/shard_map/all_gather | solution.py:35
  124.9 5.1 %fusion.80 = f32[1024,448]{0,1:T(8,128)S(1)} fusion(bf16[2048,896]{0,1:T(8,128)(2,1)} %all-gather.10.cloned.1.call-done, bf16[1024,2048]{1,0:T(8,128)(2,1)} %all-gather.8.cloned.1.call-done, f32[2048]{0:T(1024)S(1)} %copy-done.16, f32[1024]{0:T(1024)S(1)} %add_rsqrt_fusion.3), kind=kOutput, calls=%fused_computation.113 | convolution fusion | flops 1887436800 | bytes 7876608 | tf_op jit(solution)/shard_map/dot_general | solution.py:79
  130.0 2.5 fusion.91
  132.7 34.0 %all_to_all.69 = bf16[8,128,448]{1,2,0:T(8,128)(2,1)S(1)} all-to-all(bf16[8,128,448]{1,2,0:T(8,128)(2,1)S(1)} %bitcast.46), channel_id=1, replica_groups=mesh['rep'=2,'fs'=16,'tp'=8] {'tp'}, dimensions={0} | all-to-all | bytes 1835008 | tf_op jit(solution)/shard_map/all_to_all | solution.py:63
  166.8 54.7 %all-gather.12.cloned.1.call-done = bf16[3584,2048]{1,0:T(8,128)(2,1)} async-done(((bf16[448,2048]{1,0:T(8,128)(2,1)}), bf16[3584,2048]{1,0:T(8,128)(2,1)}) %all-gather.12.cloned.1.call-update) | async-done | bytes 14680080 | tf_op jit(solution)/shard_map/all_gather | solution.py:62
  221.4 2.1 fusion.61
  223.5 2.4 fusion.60
  225.9 2.6 fusion.58
  228.5 2.0 fusion.56
  230.5 0.5 fusion.54
  231.0 0.5 fusion.52
  231.5 0.5 fusion.50
  232.0 1.3 fusion.48
  233.4 0.7 pad_maximum_fusion.1
  234.4 32.1 %all_to_all.70 = bf16[16,256,128]{1,2,0:T(8,128)(2,1)} all-to-all(bf16[16,256,128]{1,2,0:T(8,128)(2,1)S(1)} %broadcast_in_dim.21), channel_id=1, replica_groups=mesh['rep'=2,'fs'=16,'tp'=8] {'fs'}, dimensions={0} | all-to-all | bytes 2097152 | tf_op jit(solution)/shard_map/all_to_all | solution.py:15
  266.6 3.1 fusion.3
  269.7 70.9 %all-gather.16.cloned.1.call-done = bf16[2048,512]{1,0:T(8,128)(2,1)} async-done(((bf16[128,512]{1,0:T(8,128)(2,1)}), bf16[2048,512]{1,0:T(8,128)(2,1)}) %all-gather.16.cloned.1.call-update) | async-done | bytes 2097168 | tf_op jit(solution)/shard_map/all_gather | solution.py:35
  340.6 4.1 fusion.169
  344.7 22.8 %all-reduce = (f32[1024]{0:T(1024)S(1)}, f32[1024]{0:T(1024)S(1)}) all-reduce(f32[1024]{0:T(1024)S(1)} %get-tuple-element.6, f32[1024]{0:T(1024)S(1)} %get-tuple-element.5), channel_id=1, replica_groups=mesh['rep'=2,'fs'=16,'tp'=8] {'tp'}, use_global_device_ids=true, to_apply=%region_5.6 | all-reduce | flops 2048 | bytes 16384 | tf_op jit(solution)/shard_map/psum | solution.py:101
  368.4 0.6 copy.41
  369.0 4.0 fusion.117
  373.1 1.0 copy.42
  374.1 4.1 all-to-all-start.2
  378.2 34.6 %all-gather.18.cloned.1.call-done = bf16[2048,2048]{0,1:T(8,128)(2,1)} async-done(((bf16[256,2048]{0,1:T(8,128)(2,1)}), bf16[2048,2048]{0,1:T(8,128)(2,1)}) %all-gather.18.cloned.1.call-update) | async-done | bytes 8388624 | tf_op jit(solution)/shard_map/all_gather | solution.py:62
  412.8 1.9 fusion.43
  414.7 2.1 fusion.42
  416.8 1.7 fusion.40
  418.5 0.5 fusion.38
  419.0 0.5 fusion.36
  419.5 0.5 fusion.34
  420.0 0.5 fusion.32
  420.5 1.3 fusion.30
  421.9 34.6 %all-gather.20.cloned.1.call-done = bf16[1024,2048]{1,0:T(8,128)(2,1)} async-done(((bf16[128,2048]{1,0:T(8,128)(2,1)}), bf16[1024,2048]{1,0:T(8,128)(2,1)}) %all-gather.20.cloned.1.call-update) | async-done | bytes 4194320 | tf_op jit(solution)/shard_map/all_gather | solution.py:45
  456.5 3.2 fusion.6
  459.9 4.0 fusion.78
  464.0 2.6 fusion.94
  466.8 16.7 %all_to_all.71 = bf16[8,128,448]{1,2,0:T(8,128)(2,1)S(1)} all-to-all(bf16[8,128,448]{1,2,0:T(8,128)(2,1)S(1)} %bitcast.47), channel_id=1, replica_groups=mesh['rep'=2,'fs'=16,'tp'=8] {'tp'}, dimensions={0} | all-to-all | bytes 1835008 | tf_op jit(solution)/shard_map/all_to_all | solution.py:63
  483.5 0.5 fusion.26
  484.0 0.5 fusion.25
  484.5 0.5 fusion.23
  486.4 0.5 fusion.15
  487.0 1.3 fusion.13
  (78 shorter events, 3.6 us)
Async XLA Ops:
  6.5 57.1 %all-gather.8.cloned.1.call-start = ((), (), s32[]{:S(2)}) async-start(), calls=%async_computation.5 | async-start | bytes 4718592 | tf_op jit(solution)/shard_map/all_gather | solution.py:45
  7.3 117.6 %all-gather.10.cloned.1.call-start = ((), (), s32[]{:S(2)}) async-start(), calls=%async_computation.6 | async-start | bytes 3899392 | tf_op jit(solution)/shard_map/all_gather | solution.py:35
  9.0 212.4 %all-gather.12.cloned.1.call-start = ((), (), s32[]{:S(2)}) async-start(), calls=%async_computation.7 | async-start | bytes 16515072 | tf_op jit(solution)/shard_map/all_gather | solution.py:62
  62.1 62.8 %copy-start.16 = (f32[2048]{0:T(1024)S(1)}, f32[2048]{0:T(1024)}, u32[]{:S(2)}) copy-start(f32[2048]{0:T(1024)} %param.15) | copy-start | bytes 24580
  63.6 203.0 %all-gather.14.cloned.1.call-start = ((), (), s32[]{:S(2)}) async-start(), calls=%async_computation.8 | async-start | bytes 4718592 | tf_op jit(solution)/shard_map/all_gather | solution.py:96
  124.9 5.1 %copy-start.4 = (bf16[1024,2048]{1,0:T(8,128)(2,1)S(1)}, bf16[1024,2048]{1,0:T(8,128)(2,1)}, u32[]{:S(2)}) copy-start(bf16[1024,2048]{1,0:T(8,128)(2,1)} %all-gather.8.cloned.1.call-done) | copy-start | bytes 12582916
  124.9 5.1 %copy-start.14 = (bf16[2048,896]{0,1:T(8,128)(2,1)S(1)}, bf16[2048,896]{0,1:T(8,128)(2,1)}, u32[]{:S(2)}) copy-start(bf16[2048,896]{0,1:T(8,128)(2,1)} %all-gather.10.cloned.1.call-done) | copy-start | bytes 11010052
  221.4 9.1 %copy-start = (bf16[3584,2048]{1,0:T(8,128)(2,1)S(1)}, bf16[3584,2048]{1,0:T(8,128)(2,1)}, u32[]{:S(2)}) copy-start(bf16[3584,2048]{1,0:T(8,128)(2,1)} %all-gather.12.cloned.1.call-done) | copy-start | bytes 44040196
  231.0 1.0 copy-start.6
  231.5 1.9 copy-start.9
  231.5 1.9 copy-start.10
  231.5 2.7 copy-start.8
  233.4 107.2 %all-gather.16.cloned.1.call-start = ((), (), s32[]{:S(2)}) async-start(), calls=%async_computation.9 | async-start | bytes 2228224 | tf_op jit(solution)/shard_map/all_gather | solution.py:35
  234.1 178.7 %all-gather.18.cloned.1.call-start = ((), (), s32[]{:S(2)}) async-start(), calls=%async_computation.10 | async-start | bytes 9437184 | tf_op jit(solution)/shard_map/all_gather | solution.py:62
  234.3 106.3 %copy-start.17 = (f32[2048]{0:T(1024)S(1)}, f32[2048]{0:T(1024)}, u32[]{:S(2)}) copy-start(f32[2048]{0:T(1024)} %param.20) | copy-start | bytes 24580
  269.6 97.9 %copy-start.11 = (f32[256]{0:T(256)S(1)}, f32[256]{0:T(256)}, u32[]{:S(2)}) copy-start(f32[256]{0:T(256)} %param.24) | copy-start | bytes 3076
  269.7 97.9 %copy-start.12 = (f32[256]{0:T(256)S(1)}, f32[256]{0:T(256)}, u32[]{:S(2)}) copy-start(f32[256]{0:T(256)} %param.23) | copy-start | bytes 3076
  269.7 98.4 %copy-start.7 = (bf16[2,128,128]{2,1,0:T(8,128)(2,1)S(1)}, bf16[2,128,128]{2,1,0:T(8,128)(2,1)}, u32[]{:S(2)}) copy-start(bf16[2,128,128]{2,1,0:T(8,128)(2,1)} %param.25) | copy-start | bytes 196612
  269.7 98.3 %copy-start.13 = (f32[2,128]{1,0:T(2,128)S(1)}, f32[2,128]{1,0:T(2,128)}, u32[]{:S(2)}) copy-start(f32[2,128]{1,0:T(2,128)} %param.26) | copy-start | bytes 3076
  374.1 38.7 %all-to-all-start.2 = ((bf16[8,128,256]{1,2,0:T(8,128)(2,1)}), bf16[8,128,256]{1,2,0:T(8,128)(2,1)S(1)}, u32[]{:S(2)}, u32[]{:S(2)}) async-start(bf16[8,128,256]{1,2,0:T(8,128)(2,1)} %copy.42), calls=%async_computation.2 | async-start | bytes 1048576 | tf_op jit(solution)/shard_map/all_to_all | solution.py:63
  378.2 78.3 %all-gather.20.cloned.1.call-start = ((), (), s32[]{:S(2)}) async-start(), calls=%async_computation.11 | async-start | bytes 4718592 | tf_op jit(solution)/shard_map/all_gather | solution.py:45
  412.8 5.7 %copy-start.1 = (bf16[2048,2048]{0,1:T(8,128)(2,1)S(1)}, bf16[2048,2048]{0,1:T(8,128)(2,1)}, u32[]{:S(2)}) copy-start(bf16[2048,2048]{0,1:T(8,128)(2,1)} %all-gather.18.cloned.1.call-done) | copy-start | bytes 25165828
  419.0 1.5 copy-start.2
  420.5 39.2 %copy-start.18 = (f32[2048]{0:T(1024)S(1)}, f32[2048]{0:T(1024)}, u32[]{:S(2)}) copy-start(f32[2048]{0:T(1024)} %param.16) | copy-start | bytes 24580
  456.5 3.4 copy-start.5
  459.9 4.0 copy-start.15
  459.9 23.5 %slice-start = ((s8[14680064]{0:T(1024)(128)(4,1)}), s8[4194304]{0:T(1024)(128)(4,1)S(1)}, s32[]{:S(2)}) async-start(s8[14680064]{0:T(1024)(128)(4,1)} %bitcast.43), calls=%async_computation.12 | async-start | bytes 8388608
  459.9 23.5 %slice-start.1 = ((s8[14680064]{0:T(1024)(128)(4,1)}), s8[4194304]{0:T(1024)(128)(4,1)S(1)}, s32[]{:S(2)}) async-start(s8[14680064]{0:T(1024)(128)(4,1)} %bitcast.43), calls=%async_computation.13 | async-start | bytes 8388608
  463.9 19.5 %slice-start.2 = ((s8[14680064]{0:T(1024)(128)(4,1)}), s8[4194304]{0:T(1024)(128)(4,1)S(1)}, s32[]{:S(2)}) async-start(s8[14680064]{0:T(1024)(128)(4,1)} %bitcast.43), calls=%async_computation.14 | async-start | bytes 8388608
  464.0 19.5 %slice-start.3 = ((s8[14680064]{0:T(1024)(128)(4,1)}), s8[2097152]{0:T(1024)(128)(4,1)S(1)}, s32[]{:S(2)}) async-start(s8[14680064]{0:T(1024)(128)(4,1)} %bitcast.43), calls=%async_computation.15 | async-start | bytes 4194304
  485.9 1.0 copy-start.3
Sparse Core Ops, SparseCore 0:
  9.2 38.7 all-gather.7
  49.7 75.1 all-gather.9
  126.7 94.6 all-gather.11
  233.5 33.0 all-gather.13
  268.2 72.3 all-gather.15
  342.2 70.5 all-gather.17
  422.0 34.4 all-gather.19
where the time goes:
time: 496 us; the launch traced here: 495 us
  waiting for transfers between devices  254 us (51%)
  blocking collectives  157 us (32%)
  matrix products  48 us (10%)
  between operations  14 us (3%)
  other arithmetic  12.1 us (2%)
  local copies, waits for them, and re-layouts  5.48 us (1%)
    all_gather x2, waiting for transfers between devices, side_by_side(): lax.all_gather(both, axis, axis=dim, tiled=True)  129 us
    all_gather x2, waiting for transfers between devices, rows_project(): weight_whole = lax.all_gather(weight_cols, 'tp', axis=0, tiled=True)  89.3 us
    all_to_all x2, blocking collectives, sent_to_all(): return lax.all_to_all(copies, axis, split_axis=0, concat_axis=0, tiled=True)  83.9 us
    all_to_all x2, blocking collectives, rows_project(): lax.all_to_all(columns_here, 'tp', split_axis=0, concat_axis=1, tiled=True)  50.8 us
    all_gather x2, waiting for transfers between devices, gathered_norm(): gathered = lax.all_gather(stream_rows, 'tp', axis=0, tiled=True)  34.6 us
    dot_general x24, matrix products, rows_project(): jnp.dot(own_tokens[:, member * width:(member + 1) * width], weight_whole[...  25.3 us
    psum x1, blocking collectives, token_mixer(): lax.psum((jnp.sum(lifted, axis=1), jnp.sum(lifted * lifted, axis=1)), 'tp')  22.8 us
  transfers between devices with their start and end apart: 8, of which 5 were waited for; matrix products, arithmetic and copies ran while one was open for 6% of the time, Pallas kernels for 0%

commit v1 on v0

--- a/solution.py
+++ b/solution.py
@@ -59,7 +59,11 @@
 
 def rows_project(columns_here, weight_shard):
     weight_cols = gathered_copies(weight_shard, "fs", 1)
-    weight_whole = lax.all_gather(weight_cols, "tp", axis=0, tiled=True)
+    n_slots = lax.psum(1, "tp")
+    pages = [n_slots if k == 0 else 1 for k in range(weight_cols.ndim)]
+    weight_whole = lax.all_to_all(
+        jnp.tile(weight_cols, pages), "tp", split_axis=0, concat_axis=0, tiled=True
+    )
     own_tokens = lax.all_to_all(columns_here, "tp", split_axis=0, concat_axis=1, tiled=True)
     width = columns_here.shape[1]
     running = jnp.zeros((own_tokens.shape[0], weight_whole.shape[1]), jnp.float32)

time: 496 us -> 585 us (1.18)
  blocking collectives: 157 us -> 249 us
  waiting for transfers between devices: 254 us -> 215 us
  starting transfers between devices: 4.31 us -> 32.2 us
  local copies, waits for them, and re-layouts: 5.48 us -> 17.4 us
    all_to_all x0 -> x1, blocking collectives: none -> 165 us  [rows_project(): lax.all_to_all(jnp.tile(weight_cols, pages), 'tp', split_axis=0, concat_a...]
    all_gather x2 -> x0, waiting for transfers between devices: 89.3 us -> none  [rows_project(): weight_whole = lax.all_gather(weight_cols, 'tp', axis=0, tiled=True)]
    all_to_all x2 -> x1, blocking collectives: 83.9 us -> 31.1 us  [sent_to_all(): return lax.all_to_all(copies, axis, split_axis=0, concat_axis=0, tiled=True)]
    all_gather x2, waiting for transfers between devices: 34.6 us -> 58.6 us  [gathered_norm(): gathered = lax.all_gather(stream_rows, 'tp', axis=0, tiled=True)]
    all_to_all x2, blocking collectives: 50.8 us -> 29.5 us  [rows_project(): lax.all_to_all(columns_here, 'tp', split_axis=0, concat_axis=1, tiled=True)]
    all_to_all x0 -> x2, starting transfers between devices: none -> 17 us  [the longest x1 9.31 us: sent_to_all(): return lax.all_to_all(copies, axis, split_axis=0, concat_axis=0, tiled=True)]
    all_gather x2, waiting for transfers between devices: 129 us -> 144 us  [side_by_side(): lax.all_gather(both, axis, axis=dim, tiled=True)]
    all_to_all x1, waiting for transfers between devices: 0.01 us -> 12 us  [rows_project(): lax.all_to_all(columns_here, 'tp', split_axis=0, concat_axis=1, tiled=True)]
where the time goes in v1:
time: 585 us; the launch traced here: 584 us
  blocking collectives  249 us (43%)
  waiting for transfers between devices  215 us (37%)
  matrix products  45.3 us (8%)
  starting transfers between devices  32.2 us (6%)
  local copies, waits for them, and re-layouts  17.4 us (3%)
  between operations  13.6 us (2%)
  other arithmetic  12.1 us (2%)
    all_to_all x1, blocking collectives, rows_project(): lax.all_to_all(jnp.tile(weight_cols, pages), 'tp', split_axis=0, concat_a...  165 us
    all_gather x2, waiting for transfers between devices, side_by_side(): lax.all_gather(both, axis, axis=dim, tiled=True)  144 us
    all_gather x2, waiting for transfers between devices, gathered_norm(): gathered = lax.all_gather(stream_rows, 'tp', axis=0, tiled=True)  58.6 us
    all_to_all x1, blocking collectives, sent_to_all(): return lax.all_to_all(copies, axis, split_axis=0, concat_axis=0, tiled=True)  31.1 us
    all_to_all x2, blocking collectives, rows_project(): lax.all_to_all(columns_here, 'tp', split_axis=0, concat_axis=1, tiled=True)  29.5 us
    psum x1, blocking collectives, token_mixer(): lax.psum((jnp.sum(lifted, axis=1), jnp.sum(lifted * lifted, axis=1)), 'tp')  23.6 us
    dot_general x24, matrix products, rows_project(): jnp.dot(own_tokens[:, member * width:(member + 1) * width], weight_whole[...  22.6 us
    all_to_all x1, starting transfers between devices, rows_project(): lax.all_to_all(columns_here, 'tp', split_axis=0, concat_axis=1, tiled=True)  14.9 us
  transfers between devices with their start and end apart: 8, of which 5 were waited for; matrix products, arithmetic and copies ran while one was open for 6% of the time, Pallas kernels for 0%

profile of v1, /device:TPU:1, one launch (start us, length us, event | category | flops | bytes accessed | tf_op | source)
XLA Modules:
  0.0 584.4 jit_solution(6432731403862925931)
XLA Ops:
  6.5 0.7 all-gather.6.cloned.1.call-update
  7.3 1.7 pad_maximum_fusion
  9.0 2.5 broadcast_in_dim.14
  11.5 9.3 %all-to-all-start.1 = ((bf16[16,448,128]{2,1,0:T(8,128)(2,1)}), bf16[16,448,128]{2,1,0:T(8,128)(2,1)S(1)}, u32[]{:S(2)}, u32[]{:S(2)}) async-start(bf16[16,448,128]{2,1,0:T(8,128)(2,1)} %broadcast_in_dim.14), calls=%async_computation.1 | async-start | bytes 3670016 | tf_op jit(solution)/shard_map/all_to_all | solution.py:15
  20.8 27.2 %all-gather.6.cloned.1.call-done = bf16[1024,2048]{1,0:T(8,128)(2,1)} async-done(((bf16[128,2048]{1,0:T(8,128)(2,1)}), bf16[1024,2048]{1,0:T(8,128)(2,1)}) %all-gather.6.cloned.1.call-update) | async-done | bytes 4194320 | tf_op jit(solution)/shard_map/all_gather | solution.py:45
  48.0 3.1 fusion
  51.1 74.4 %all-gather.8.cloned.1.call-done = bf16[2048,896]{0,1:T(8,128)(2,1)} async-done(((bf16[128,896]{0,1:T(8,128)(2,1)}), bf16[2048,896]{0,1:T(8,128)(2,1)}) %all-gather.8.cloned.1.call-update) | async-done | bytes 3670032 | tf_op jit(solution)/shard_map/all_gather | solution.py:35
  125.5 5.1 fusion.64
  130.6 2.5 fusion.75
  133.1 1.1 copy.60
  134.2 14.9 %all-to-all-start = ((bf16[8,128,448]{1,2,0:T(8,128)(2,1)}), bf16[8,128,448]{1,2,0:T(8,128)(2,1)S(1)}, u32[]{:S(2)}, u32[]{:S(2)}) async-start(bf16[8,128,448]{1,2,0:T(8,128)(2,1)} %bitcast.98), calls=%async_computation | async-start | bytes 1835008 | tf_op jit(solution)/shard_map/all_to_all | solution.py:67
  149.1 1.5 copy_bitcast_fusion
  150.7 12.0 %all-to-all-done = bf16[8,128,448]{1,2,0:T(8,128)(2,1)S(1)} async-done(((bf16[8,128,448]{1,2,0:T(8,128)(2,1)}), bf16[8,128,448]{1,2,0:T(8,128)(2,1)S(1)}, u32[]{:S(2)}, u32[]{:S(2)}) %all-to-all-start) | async-done | bytes 917536 | tf_op jit(solution)/shard_map/all_to_all | solution.py:67
  162.7 3.7 tile.9
  166.4 164.7 %all_to_all.81 = bf16[8,448,2048]{2,1,0:T(8,128)(2,1)S(1)} all-to-all(bf16[8,448,2048]{2,1,0:T(8,128)(2,1)S(1)} %tile.9), channel_id=1, replica_groups=mesh['rep'=2,'fs'=16,'tp'=8] {'tp'}, dimensions={0} | all-to-all | bytes 29360128 | tf_op jit(solution)/shard_map/all_to_all | solution.py:64
  331.5 0.5 fusion.60
  332.0 0.5 fusion.58
  332.5 0.5 fusion.56
  333.0 0.5 fusion.54
  333.5 0.5 fusion.52
  334.5 1.8 copy-done
  336.2 1.3 fusion.48
  337.8 31.1 %all_to_all.82 = bf16[16,256,128]{1,2,0:T(8,128)(2,1)S(1)} all-to-all(bf16[16,256,128]{1,2,0:T(8,128)(2,1)S(1)} %broadcast_in_dim.21), channel_id=1, replica_groups=mesh['rep'=2,'fs'=16,'tp'=8] {'fs'}, dimensions={0} | all-to-all | bytes 2097152 | tf_op jit(solution)/shard_map/all_to_all | solution.py:15
  368.9 0.6 copy.45
  369.6 4.4 tile.11
  373.9 7.7 %all-to-all-start.5 = ((bf16[8,256,2048]{2,1,0:T(8,128)(2,1)}), bf16[8,256,2048]{2,1,0:T(8,128)(2,1)}, u32[]{:S(2)}, u32[]{:S(2)}) async-start(bf16[8,256,2048]{2,1,0:T(8,128)(2,1)} %tile.11), calls=%async_computation.5 | async-start | bytes 16777216 | tf_op jit(solution)/shard_map/all_to_all | solution.py:64
  381.6 0.7 pad_maximum_fusion.1
  382.6 3.1 fusion.3
  385.8 69.1 %all-gather.12.cloned.1.call-done = bf16[2048,512]{1,0:T(8,128)(2,1)} async-done(((bf16[128,512]{1,0:T(8,128)(2,1)}), bf16[2048,512]{1,0:T(8,128)(2,1)}) %all-gather.12.cloned.1.call-update) | async-done | bytes 2097168 | tf_op jit(solution)/shard_map/all_gather | solution.py:35
  454.9 4.1 fusion.145
  459.0 23.6 %all-reduce = (f32[1024]{0:T(1024)S(1)}, f32[1024]{0:T(1024)S(1)}) all-reduce(f32[1024]{0:T(1024)S(1)} %get-tuple-element.6, f32[1024]{0:T(1024)S(1)} %get-tuple-element.5), channel_id=1, replica_groups=mesh['rep'=2,'fs'=16,'tp'=8] {'tp'}, use_global_device_ids=true, to_apply=%region_5.6 | all-reduce | flops 2048 | bytes 16384 | tf_op jit(solution)/shard_map/psum | solution.py:105
  483.5 0.6 copy.42
  484.1 4.0 fusion.101
  488.4 12.8 %all_to_all.83 = bf16[8,128,256]{1,2,0:T(8,128)(2,1)S(1)} all-to-all(bf16[8,128,256]{1,2,0:T(8,128)(2,1)S(1)} %copy.43), channel_id=1, replica_groups=mesh['rep'=2,'fs'=16,'tp'=8] {'tp'}, dimensions={0} | all-to-all | bytes 1048576 | tf_op jit(solution)/shard_map/all_to_all | solution.py:67
  501.2 1.6 fusion.43
  502.8 1.6 fusion.42
  504.4 1.6 fusion.40
  505.9 1.6 fusion.38
  507.5 1.6 fusion.36
  509.1 1.6 fusion.34
  510.7 1.6 fusion.32
  512.3 2.4 fusion.30
  514.7 31.4 %all-gather.14.cloned.1.call-done = bf16[1024,2048]{1,0:T(8,128)(2,1)} async-done(((bf16[128,2048]{1,0:T(8,128)(2,1)}), bf16[1024,2048]{1,0:T(8,128)(2,1)}) %all-gather.14.cloned.1.call-update) | async-done | bytes 4194320 | tf_op jit(solution)/shard_map/all_gather | solution.py:45
  546.1 3.2 fusion.6
  549.5 4.0 fusion.62
  553.6 2.6 fusion.78
  556.4 16.7 %all_to_all.84 = bf16[8,128,448]{1,2,0:T(8,128)(2,1)S(1)} all-to-all(bf16[8,128,448]{1,2,0:T(8,128)(2,1)S(1)} %bitcast.102), channel_id=1, replica_groups=mesh['rep'=2,'fs'=16,'tp'=8] {'tp'}, dimensions={0} | all-to-all | bytes 1835008 | tf_op jit(solution)/shard_map/all_to_all | solution.py:67
  576.6 1.3 fusion.13
  (77 shorter events, 6.5 us)
Async XLA Ops:
  6.5 41.5 %all-gather.6.cloned.1.call-start = ((), (), s32[]{:S(2)}) async-start(), calls=%async_computation.7 | async-start | bytes 4718592 | tf_op jit(solution)/shard_map/all_gather | solution.py:45
  7.3 118.2 %all-gather.8.cloned.1.call-start = ((), (), s32[]{:S(2)}) async-start(), calls=%async_computation.8 | async-start | bytes 3899392 | tf_op jit(solution)/shard_map/all_gather | solution.py:35
  11.5 113.9 %copy-start.15 = (f32[2048]{0:T(1024)S(1)}, f32[2048]{0:T(1024)}, u32[]{:S(2)}) copy-start(f32[2048]{0:T(1024)} %param.15) | copy-start | bytes 24580
  11.5 122.7 %all-to-all-start.1 = ((bf16[16,448,128]{2,1,0:T(8,128)(2,1)}), bf16[16,448,128]{2,1,0:T(8,128)(2,1)S(1)}, u32[]{:S(2)}, u32[]{:S(2)}) async-start(bf16[16,448,128]{2,1,0:T(8,128)(2,1)} %broadcast_in_dim.14), calls=%async_computation.1 | async-start | bytes 3670016 | tf_op jit(solution)/shard_map/all_to_all | solution.py:15
  125.5 5.1 copy-start.3
  125.5 5.1 copy-start.13
  134.2 28.5 %all-to-all-start = ((bf16[8,128,448]{1,2,0:T(8,128)(2,1)}), bf16[8,128,448]{1,2,0:T(8,128)(2,1)S(1)}, u32[]{:S(2)}, u32[]{:S(2)}) async-start(bf16[8,128,448]{1,2,0:T(8,128)(2,1)} %bitcast.98), calls=%async_computation | async-start | bytes 1835008 | tf_op jit(solution)/shard_map/all_to_all | solution.py:67
  149.1 233.5 %all-gather.10.cloned.1.call-start = ((), (), s32[]{:S(2)}) async-start(), calls=%async_computation.9 | async-start | bytes 4718592 | tf_op jit(solution)/shard_map/all_gather | solution.py:100
  331.1 5.2 copy-start
  333.5 2.8 copy-start.5
  334.0 3.6 copy-start.7
  373.9 7.7 %copy-start.8 = (bf16[128,256]{1,0:T(8,128)(2,1)S(1)}, bf16[128,256]{1,0:T(8,128)(2,1)}, u32[]{:S(2)}) copy-start(bf16[128,256]{1,0:T(8,128)(2,1)} %param.22) | copy-start | bytes 196612
  373.9 7.7 %copy-start.9 = (bf16[128,256]{1,0:T(8,128)(2,1)S(1)}, bf16[128,256]{1,0:T(8,128)(2,1)}, u32[]{:S(2)}) copy-start(bf16[128,256]{1,0:T(8,128)(2,1)} %param.21) | copy-start | bytes 196612
  373.9 114.5 %all-to-all-start.5 = ((bf16[8,256,2048]{2,1,0:T(8,128)(2,1)}), bf16[8,256,2048]{2,1,0:T(8,128)(2,1)}, u32[]{:S(2)}, u32[]{:S(2)}) async-start(bf16[8,256,2048]{2,1,0:T(8,128)(2,1)} %tile.11), calls=%async_computation.5 | async-start | bytes 16777216 | tf_op jit(solution)/shard_map/all_to_all | solution.py:64
  381.6 73.2 %copy-start.16 = (f32[2048]{0:T(1024)S(1)}, f32[2048]{0:T(1024)}, u32[]{:S(2)}) copy-start(f32[2048]{0:T(1024)} %param.20) | copy-start | bytes 24580
  381.6 73.2 %all-gather.12.cloned.1.call-start = ((), (), s32[]{:S(2)}) async-start(), calls=%async_computation.10 | async-start | bytes 2228224 | tf_op jit(solution)/shard_map/all_gather | solution.py:35
  382.3 163.8 %all-gather.14.cloned.1.call-start = ((), (), s32[]{:S(2)}) async-start(), calls=%async_computation.11 | async-start | bytes 4718592 | tf_op jit(solution)/shard_map/all_gather | solution.py:45
  385.7 96.9 %copy-start.10 = (f32[256]{0:T(256)S(1)}, f32[256]{0:T(256)}, u32[]{:S(2)}) copy-start(f32[256]{0:T(256)} %param.24) | copy-start | bytes 3076
  385.7 96.9 %copy-start.11 = (f32[256]{0:T(256)S(1)}, f32[256]{0:T(256)}, u32[]{:S(2)}) copy-start(f32[256]{0:T(256)} %param.23) | copy-start | bytes 3076
  385.7 97.4 %copy-start.6 = (bf16[2,128,128]{2,1,0:T(8,128)(2,1)S(1)}, bf16[2,128,128]{2,1,0:T(8,128)(2,1)}, u32[]{:S(2)}) copy-start(bf16[2,128,128]{2,1,0:T(8,128)(2,1)} %param.25) | copy-start | bytes 196612
  385.7 97.4 %copy-start.12 = (f32[2,128]{1,0:T(2,128)S(1)}, f32[2,128]{1,0:T(2,128)}, u32[]{:S(2)}) copy-start(f32[2,128]{1,0:T(2,128)} %param.26) | copy-start | bytes 3076
  507.5 4.8 copy-start.1
  512.3 37.1 %copy-start.17 = (f32[2048]{0:T(1024)S(1)}, f32[2048]{0:T(1024)}, u32[]{:S(2)}) copy-start(f32[2048]{0:T(1024)} %param.16) | copy-start | bytes 24580
  546.1 3.4 copy-start.4
  549.5 4.0 copy-start.14
  549.5 23.6 %slice-start = ((s8[14680064]{0:T(1024)(128)(4,1)}), s8[4194304]{0:T(1024)(128)(4,1)S(1)}, s32[]{:S(2)}) async-start(s8[14680064]{0:T(1024)(128)(4,1)} %bitcast.99), calls=%async_computation.12 | async-start | bytes 8388608
  549.5 23.6 %slice-start.1 = ((s8[14680064]{0:T(1024)(128)(4,1)}), s8[4194304]{0:T(1024)(128)(4,1)S(1)}, s32[]{:S(2)}) async-start(s8[14680064]{0:T(1024)(128)(4,1)} %bitcast.99), calls=%async_computation.13 | async-start | bytes 8388608
  553.6 19.6 %slice-start.2 = ((s8[14680064]{0:T(1024)(128)(4,1)}), s8[4194304]{0:T(1024)(128)(4,1)S(1)}, s32[]{:S(2)}) async-start(s8[14680064]{0:T(1024)(128)(4,1)} %bitcast.99), calls=%async_computation.14 | async-start | bytes 8388608
  553.6 19.6 %slice-start.3 = ((s8[14680064]{0:T(1024)(128)(4,1)}), s8[2097152]{0:T(1024)(128)(4,1)S(1)}, s32[]{:S(2)}) async-start(s8[14680064]{0:T(1024)(128)(4,1)} %bitcast.99), calls=%async_computation.15 | async-start | bytes 4194304
  575.5 1.0 copy-start.2
Sparse Core Ops, SparseCore 0:
  9.2 38.7 all-gather.5
  49.7 75.7 all-gather.7
  337.7 34.8 all-gather.9
  383.9 70.9 all-gather.11
  514.8 31.2 all-gather.13
